TPU v7x, 512 devices: a whole 4x4x16 slice. The times are simulated.
512 devices in a mesh: ep: 32 (over z, core), tp: 16 (over y, x).
Axes of the slice: x: 4, y: 4, z: 16, core: 2. Of those that a mesh axis runs over, the one named last changes fastest.
Arguments:
- queries: bfloat16 [8192, 2048], P('ep', 'tp'), may hold values from -6 to 6
- keys: bfloat16 [8192, 2048], P('ep', 'tp'), may hold values from -6 to 6
- values: bfloat16 [8192, 2048], P('ep', 'tp'), may hold values from -6 to 6
- gates: bfloat16 [8192, 2048], P('ep', 'tp'), may hold values from -6 to 6
- log_decay: float32 [8192, 16], P('ep', 'tp'), may hold values from -2 to 0
- out_weight: bfloat16 [2048, 2048], P(None, 'tp'), may hold values from -0.125 to 0.125
- moe_rows: bfloat16 [8192, 2048], P('ep'), may hold values from -140 to 140
- moe_gain: bfloat16 [2048], replicated, may hold values from 0.099609375 to 1.8984375
- routes: int32 [8192, 2], P('ep'), may hold values from 0 to 31, as said below
- route_weights: float32 [8192, 2], P('ep'), may hold values from 0.1 to 1
- gate_proj: bfloat16 [32, 2048, 4096], P('ep', None, 'tp'), may hold values from -0.125 to 0.125
- up_proj: bfloat16 [32, 2048, 4096], P('ep', None, 'tp'), may hold values from -0.125 to 0.125
- down_proj: bfloat16 [32, 4096, 2048], P('ep', None, 'tp'), may hold values from -0.09375 to 0.09375
Outputs:
- mixer_out: bfloat16 [8192, 2048], P('ep', 'tp')
- moe_out: bfloat16 [8192, 2048], P('ep', 'tp')
Inputs may be any that keep to these rules, and one draw needn't show every extreme that they name: `routes`: each row names two different experts of one group of 8 consecutive experts; in each aligned block of 256 rows every expert is named by exactly 16 rows.
All inputs are finite; a program needn't handle non-finite values.
Results may differ from a plain program's by a relative error of at most 0.011.
Values may be sent and summed in bfloat16 or wider, within the bound.
No kernel may reach another device: no remote copies, remote signals or barrier semaphores. Data moves between devices by JAX's collectives and lax.ppermute only.
A program may use at most 64 MiB of HBM per device.

v0:
```python
import jax
import jax.numpy as jnp
from jax import lax
from jax.sharding import Mesh
from jax.sharding import PartitionSpec as P

BLOCK = 128
EP = ("ep_0", "ep_1")
TP = ("tp_0", "tp_1")


def filled_with(array, identity):
    return jax.tree.map(
        lambda part, zero: jnp.zeros_like(part) + jnp.asarray(zero, part.dtype), array, identity
    )


def collected_together(array, axis):
    leaves = jax.tree.leaves(array)
    turns = sorted(range(len(leaves)), key=lambda k: -leaves[k].size)
    width = (1, *leaves[turns[0]].shape)[-1]
    lines = [
        jnp.pad(leaves[k].reshape(-1), (0, -leaves[k].size % width)).reshape(-1, width)
        for k in turns
    ]
    both, at, found = (lax.all_gather(jnp.concatenate(lines), axis), 0, {})
    for k, line in zip(turns, lines):
        piece = both[:, at : at + len(line)].reshape(len(both), -1)
        found[k] = piece[:, : leaves[k].size].reshape(-1, *leaves[k].shape)
        at += len(line)
    numbers = iter(range(len(leaves)))
    return jax.tree.map(lambda _: found[next(numbers)], array)


def carried_in(array, axes, combine, identity):
    before = start = filled_with(array, identity)
    total = array
    for axis in reversed(axes):
        peers, mine = (lax.axis_size(axis), lax.axis_index(axis))
        pieces = collected_together(total, axis)
        inside, total = (start, start)
        for k in range(peers):
            passed = k < mine
            total = combine(total, jax.tree.map(lambda part: part[k], pieces))
            inside = jax.tree.map(lambda new, old: jnp.where(passed, new, old), total, inside)
        before = combine(inside, before)
    return before


def whole_of(array, axes, dim):
    for axis in reversed(axes):
        array = lax.all_gather(array, axis, axis=dim, tiled=True)
    return array


def in_order(parts, dim):
    lengths = list(parts.shape[1:])
    lengths[dim] *= parts.shape[0]
    return jnp.moveaxis(parts, 0, dim).reshape(lengths)


def copy_for_each(array, axis):
    peers = lax.axis_size(axis)
    return lax.all_to_all(
        jnp.broadcast_to(array[None], (peers, *array.shape)), axis, 0, 0, tiled=True
    )


def collect(array, axis, dim):
    return in_order(copy_for_each(array, axis), dim)


def rotate(source, positions, heads_here, factor):
    row_count, feat_width = source.shape
    head_dim = feat_width // heads_here
    half_dim = head_dim // 2
    values_f = source.astype(jnp.float32).reshape(row_count, heads_here, head_dim)
    inverse = 10000.0 ** (-jnp.arange(half_dim, dtype=jnp.float32) / half_dim)
    angles = positions[:, None] * inverse[None, :]
    cosine = jnp.cos(angles)[:, None, :]
    sine_part = jnp.sin(angles)[:, None, :]
    first_half = values_f[..., :half_dim]
    second_half = values_f[..., half_dim:]
    turned = jnp.concatenate(
        [
            first_half * cosine - second_half * sine_part,
            first_half * sine_part + second_half * cosine,
        ],
        axis=-1,
    )
    return (turned * factor).astype(jnp.bfloat16).reshape(row_count, feat_width)


def chain_states(earlier, later):
    return (earlier[0] * later[0], later[0][:, None, None] * earlier[1] + later[1])


def retention_half(queries, keys, values, gates, log_decay, out_weight):
    row_count, feat_width = queries.shape
    heads_here = log_decay.shape[1]
    head_dim = feat_width // heads_here
    block_count = row_count // BLOCK
    positions = (lax.axis_index(EP) * row_count + jnp.arange(row_count, dtype=jnp.int32)).astype(
        jnp.float32
    )
    rot_q = rotate(queries, positions, heads_here, 1.0)
    rot_k = rotate(keys, positions, heads_here, head_dim ** (-0.5))
    block_shape = (block_count, BLOCK, heads_here, head_dim)
    q_blocks = rot_q.reshape(block_shape)
    k_blocks = rot_k.reshape(block_shape)
    v_blocks = values.reshape(block_shape)
    cumulative = jnp.cumsum(log_decay.reshape(block_count, BLOCK, heads_here), axis=1)
    across = jnp.swapaxes(cumulative, 1, 2)
    spread = across[..., :, None] - across[..., None, :]
    causal = jnp.arange(BLOCK)[:, None] >= jnp.arange(BLOCK)[None, :]
    weights = jnp.where(causal, jnp.exp(jnp.where(causal, spread, 0.0)), 0.0)
    scores = jnp.einsum("nihd,njhd->nhij", q_blocks, k_blocks, preferred_element_type=jnp.float32)
    rounded = (scores * weights).astype(jnp.bfloat16)
    inside = jnp.einsum("nhij,njhd->nihd", rounded, v_blocks, preferred_element_type=jnp.float32)
    ending = cumulative[:, -1, :]
    k_scaled = k_blocks.astype(jnp.float32) * jnp.exp(ending[:, None, :] - cumulative)[..., None]
    updates = jnp.einsum(
        "njhd,njhe->nhde", k_scaled, v_blocks.astype(jnp.float32), precision=lax.Precision.HIGHEST
    )

    def advance(carry_state, member):
        return (jnp.exp(member[0])[:, None, None] * carry_state + member[1], carry_state)

    zero_state = jnp.zeros((heads_here, head_dim, head_dim), jnp.float32)
    local_end, before = lax.scan(advance, zero_state, (ending, updates))
    device_decay = jnp.exp(jnp.sum(ending, axis=0))
    incoming = carried_in(
        (device_decay, local_end), EP, chain_states, (jnp.ones_like(device_decay), zero_state)
    )
    leading = jnp.cumsum(ending, axis=0) - ending
    entering = before + jnp.exp(leading)[:, :, None, None] * incoming[1][None]
    carried = (
        jnp.einsum(
            "nihd,nhde->nihe",
            q_blocks.astype(jnp.float32),
            entering,
            precision=lax.Precision.HIGHEST,
        )
        * jnp.exp(cumulative)[..., None]
    )
    retained = (inside + carried).reshape(row_count, heads_here, head_dim)
    gate_f = gates.astype(jnp.float32).reshape(row_count, heads_here, head_dim)
    scaled = retained * lax.rsqrt(jnp.mean(retained * retained, axis=-1, keepdims=True) + 1e-05)
    head_out = (scaled * jax.nn.silu(gate_f)).astype(jnp.bfloat16).reshape(row_count, feat_width)
    projected = jnp.dot(whole_of(head_out, TP, 1), out_weight, preferred_element_type=jnp.float32)
    return projected.astype(jnp.bfloat16)


def expert_half(moe_rows, moe_gain, routes, route_weights, gate_proj, up_proj, down_proj):
    row_count, feat_width = moe_rows.shape
    experts = lax.axis_size(EP)
    capacity = 2 * row_count // experts
    as_float = moe_rows.astype(jnp.float32)
    normed = (
        as_float
        * lax.rsqrt(jnp.mean(as_float * as_float, axis=-1, keepdims=True) + 1e-06)
        * moe_gain.astype(jnp.float32)
    ).astype(jnp.bfloat16)
    flat_ids = routes.reshape(-1)
    onehot = (flat_ids[:, None] == jnp.arange(experts, dtype=jnp.int32)[None, :]).astype(jnp.int32)
    slot_rank = jnp.sum((jnp.cumsum(onehot, axis=0) - onehot) * onehot, axis=1)
    target = flat_ids * capacity + slot_rank
    source_row = (
        jnp.zeros((experts * capacity,), jnp.int32)
        .at[target]
        .set(jnp.arange(2 * row_count, dtype=jnp.int32) // 2)
    )
    outgoing = normed[source_row].reshape(experts, capacity, feat_width)
    w_gate = gate_proj[0]
    w_up = up_proj[0]
    w_down = down_proj[0]
    share_size = capacity // lax.axis_size(TP)
    own_share = lax.dynamic_slice_in_dim(outgoing, lax.axis_index(TP) * share_size, share_size, 1)
    arrived_share = lax.all_to_all(own_share, EP, split_axis=0, concat_axis=0, tiled=True)
    arrived = collect(arrived_share, TP, 1)
    gate_part = jnp.einsum("scd,df->scf", arrived, w_gate, preferred_element_type=jnp.float32)
    up_part = jnp.einsum("scd,df->scf", arrived, w_up, preferred_element_type=jnp.float32)
    hidden = (jax.nn.silu(gate_part) * up_part).astype(jnp.bfloat16)
    expert_out = jnp.einsum(
        "scf,fd->scd",
        lax.all_gather(hidden, TP, axis=2, tiled=True),
        w_down,
        preferred_element_type=jnp.float32,
    ).astype(jnp.bfloat16)
    returned = lax.all_to_all(expert_out, EP, split_axis=0, concat_axis=0, tiled=True)
    picked = returned.reshape(experts * capacity, -1)[target].reshape(row_count, 2, -1)
    return jnp.sum(picked.astype(jnp.float32) * route_weights[:, :, None], axis=1).astype(
        jnp.bfloat16
    )


def on_device(
    queries,
    keys,
    values,
    gates,
    log_decay,
    out_weight,
    moe_rows,
    moe_gain,
    routes,
    route_weights,
    gate_proj,
    up_proj,
    down_proj,
):
    mixer_out = retention_half(queries, keys, values, gates, log_decay, out_weight)
    moe_out = expert_half(moe_rows, moe_gain, routes, route_weights, gate_proj, up_proj, down_proj)
    return (mixer_out, moe_out)


def solution(mesh):
    torus = Mesh(mesh.devices.reshape(16, 2, 4, 4), ("ep_0", "ep_1", "tp_0", "tp_1"))
    return jax.shard_map(
        on_device,
        mesh=torus,
        in_specs=(
            P(EP, TP),
            P(EP, TP),
            P(EP, TP),
            P(EP, TP),
            P(EP, TP),
            P(None, TP),
            P(EP, None),
            P(),
            P(EP, None),
            P(EP, None),
            P(EP, None, TP),
            P(EP, None, TP),
            P(EP, None, TP),
        ),
        out_specs=(P(EP, TP), P(EP, TP)),
        check_vma=False,
    )
```

profile of v0, /device:TPU:2, one launch (start us, length us, event | category | flops | bytes accessed | tf_op | source)
XLA Modules:
  0.0 250.1 jit_solution(12538296000440214369)
XLA Ops:
  7.2 1.0 copy.44
  8.2 0.1 eq.29
  8.3 0.1 eq.25
  8.4 0.7 broadcast_multiply_fusion
  9.1 1.2 reduce-window.18
  10.3 0.2 slice_reduce_fusion
  10.6 0.1 copy.43
  10.7 0.1 mul.536
  10.9 0.1 fusion.53
  11.0 2.4 scatter_custom_fusion
  13.5 0.7 convert_element_type.89
  14.2 1.5 fusion
  15.7 0.3 fusion.2
  16.0 3.3 %gather_fusion = bf16[512,2048]{1,0:T(8,128)(2,1)} fusion(bf16[256,2048]{1,0:T(8,128)(2,1)S(1)} %fusion.2, s32[1024]{0:T(1024)S(1)} %pad_clamp_fusion.1), kind=kCustom, calls=%fused_computation | custom fusion | bytes 4196352 | tf_op jit(solution)/shard_map/gather | solution.py:173
  19.4 1.5 constant_dynamic-slice_fusion.1
  20.9 0.5 broadcast.370
  21.4 1.4 reduce.10
  22.8 0.7 reshape.656
  23.5 15.5 %all-to-all-start = ((bf16[32,2,1024]{2,1,0:T(2,128)(2,1)}), bf16[32,2,1024]{2,1,0:T(2,128)(2,1)S(1)}, u32[]{:S(2)}, u32[]{:S(2)}) async-start(bf16[32,2,1024]{2,1,0:T(2,128)(2,1)} %reshape.656), calls=%async_computation | async-start | bytes 262144 | tf_op jit(solution)/shard_map/all_to_all | solution.py:179
  39.1 0.1 copy.40
  39.2 0.2 reduce_window_sum.33
  39.4 0.6 slice_reduce_fusion.1
  40.0 0.1 reduce.4
  40.2 0.6 fusion.34
  40.8 0.1 fusion.39
  40.9 0.6 fusion.80
  41.5 0.4 convolution_bitcast_fusion.1
  41.9 2.4 while.13
  41.9 0.6 fusion.88
  42.5 0.6 bitcast_add_fusion.2
  43.1 0.6 fusion.88
  43.7 0.6 bitcast_add_fusion.2
  44.9 0.5 pad_bitcast_fusion.1
  45.5 10.7 %all-to-all-done = bf16[32,2,1024]{2,1,0:T(2,128)(2,1)S(1)} async-done(((bf16[32,2,1024]{2,1,0:T(2,128)(2,1)}), bf16[32,2,1024]{2,1,0:T(2,128)(2,1)S(1)}, u32[]{:S(2)}, u32[]{:S(2)}) %all-to-all-start) | async-done | bytes 131104 | tf_op jit(solution)/shard_map/all_to_all | solution.py:179
  56.2 0.1 reshape.657
  56.4 1.6 broadcast_in_dim.33
  58.0 7.5 %all-to-all-start.1 = ((bf16[16,32,1,2048]{3,1,2,0:T(8,128)(2,1)}), bf16[16,32,1,2048]{3,1,2,0:T(8,128)(2,1)S(1)}, u32[]{:S(2)}, u32[]{:S(2)}) async-start(bf16[16,32,1,2048]{3,1,2,0:T(8,128)(2,1)} %broadcast_in_dim.33), calls=%async_computation.1 | async-start | bytes 4194304 | tf_op jit(solution)/shard_map/all_to_all | solution.py:64
  65.6 1.9 all-gather.2
  67.5 0.6 fusion.79
  70.0 0.7 fusion.66
  70.6 0.6 maximum_bitcast_fusion.1
  71.3 20.4 %all-to-all-done.1 = bf16[16,32,1,2048]{3,1,2,0:T(8,128)(2,1)S(1)} async-done(((bf16[16,32,1,2048]{3,1,2,0:T(8,128)(2,1)}), bf16[16,32,1,2048]{3,1,2,0:T(8,128)(2,1)S(1)}, u32[]{:S(2)}, u32[]{:S(2)}) %all-to-all-start.1) | async-done | bytes 2097184 | tf_op jit(solution)/shard_map/all_to_all | solution.py:64
  91.7 0.7 fusion.5
  92.5 0.5 copy-done.12
  92.9 1.4 fusion.10
  94.5 0.9 reduce-window.14
  96.0 0.6 fusion.72
  96.6 36.7 %all-gather.12.cloned.1.call-done = f32[16,129,128]{2,1,0:T(8,128)} async-done(((f32[1,129,128]{2,1,0:T(8,128)}), f32[16,129,128]{2,1,0:T(8,128)}) %all-gather.12.cloned.1.call-update) | async-done | bytes 1056784 | tf_op jit(solution)/shard_map/all_gather | solution.py:26
  133.3 0.8 slice.250
  134.2 0.6 fusion.78
  135.4 11.5 %fusion.57 = f32[128,128]{1,0:T(8,128)S(1)} fusion(f32[16,129,128]{2,1,0:T(8,128)} %all-gather.12.cloned.1.call-done, f32[2,129,128]{2,1,0:T(8,128)S(1)} %all-gather.2, f32[]{:T(128)} %bitcast.46, f32[]{:T(128)} %bitcast.45, f32[]{:T(128)} %bitcast.44, f32[]{:T(128)} %bitcast.43, f32[]{:T(128)} %bitcast.42, f32[]{:T(128)} %bitcast.41, f32[]{:T(128)} %bitcast.40, ...), kind=kLoop, calls=%fused_computation.81 | loop fusion | flops 884736 | bytes 1245278 | tf_op jit(solution)/shard_map/mul | solution.py:136
  146.9 1.2 fusion.14
  148.1 0.4 fusion.40
  148.6 0.1 fusion.50
  148.7 13.4 %all_gather.25 = bf16[256,512]{1,0:T(8,128)(2,1)} all-gather(bf16[256,128]{1,0:T(8,128)(2,1)S(1)} %fusion.50), channel_id=1, replica_groups=mesh['ep_0'=16,'ep_1'=2,'tp_0'=4,'tp_1'=4] {'tp_1'}, dimensions={1}, use_global_device_ids=true | all-gather | bytes 327680 | tf_op jit(solution)/shard_map/all_gather | solution.py:52
  162.2 43.0 %all-gather.10.cloned.1.call-done = bf16[32,16,4096]{2,0,1:T(8,128)(2,1)} async-done(((bf16[32,16,256]{2,0,1:T(8,128)(2,1)}), bf16[32,16,4096]{2,0,1:T(8,128)(2,1)}) %all-gather.10.cloned.1.call-update) | async-done | bytes 4194320 | tf_op jit(solution)/shard_map/all_gather | solution.py:186
  205.2 3.4 %fusion.16 = bf16[32,16,128]{2,0,1:T(8,128)(2,1)S(1)} fusion(bf16[32,16,4096]{2,0,1:T(8,128)(2,1)} %all-gather.10.cloned.1.call-done, bf16[1,4096,128]{2,1,0:T(8,128)(2,1)S(1)} %copy-done.13), kind=kOutput, calls=%fused_computation.25 | convolution fusion | flops 536870912 | bytes 5373952 | tf_op jit(solution)/shard_map/scf,fd->scd/dot_general | solution.py:184
  208.6 0.7 copy.58
  209.3 12.6 %all-to-all-start.2 = ((bf16[32,16,128]{2,1,0:T(8,128)(2,1)}), bf16[32,16,128]{2,1,0:T(8,128)(2,1)S(1)}, u32[]{:S(2)}, u32[]{:S(2)}) async-start(bf16[32,16,128]{2,1,0:T(8,128)(2,1)} %copy.58), calls=%async_computation.2 | async-start | bytes 262144 | tf_op jit(solution)/shard_map/all_to_all | solution.py:190
  221.9 0.1 copy.49
  222.1 16.8 %all-gather.8.cloned.1.call-done = bf16[256,2048]{1,0:T(8,128)(2,1)} async-done(((bf16[256,512]{1,0:T(8,128)(2,1)}), bf16[256,2048]{1,0:T(8,128)(2,1)}) %all-gather.8.cloned.1.call-update) | async-done | bytes 1048592 | tf_op jit(solution)/shard_map/all_gather | solution.py:52
  238.9 2.3 convolution_convert_fusion
  241.2 1.3 gather_fusion.1
  242.5 1.1 fusion.20
  (56 shorter events, 0.5 us)
Async XLA Ops:
  7.2 84.6 %copy-start = (bf16[1,2048,256]{2,1,0:T(8,128)(2,1)S(1)}, bf16[1,2048,256]{2,1,0:T(8,128)(2,1)}, u32[]{:S(2)}) copy-start(bf16[1,2048,256]{2,1,0:T(8,128)(2,1)} %param.25) | copy-start | bytes 3145732
  7.2 8.5 %copy-start.1 = (bf16[256,2048]{1,0:T(8,128)(2,1)S(1)}, bf16[256,2048]{1,0:T(8,128)(2,1)}, u32[]{:S(2)}) copy-start(bf16[256,2048]{1,0:T(8,128)(2,1)} %param.21) | copy-start | bytes 3145732
  16.0 23.1 %copy-start.10 = (f32[256,1]{0,1:T(1,128)S(1)}, f32[256,1]{0,1:T(1,128)}, u32[]{:S(2)}) copy-start(f32[256,1]{0,1:T(1,128)} %param.19) | copy-start | bytes 3076
  16.0 24.1 %copy-start.4 = (bf16[256,128]{1,0:T(8,128)(2,1)S(1)}, bf16[256,128]{1,0:T(8,128)(2,1)}, u32[]{:S(2)}) copy-start(bf16[256,128]{1,0:T(8,128)(2,1)} %param.16) | copy-start | bytes 196612
  16.0 24.1 %copy-start.5 = (bf16[256,128]{1,0:T(8,128)(2,1)S(1)}, bf16[256,128]{1,0:T(8,128)(2,1)}, u32[]{:S(2)}) copy-start(bf16[256,128]{1,0:T(8,128)(2,1)} %param.15) | copy-start | bytes 196612
  19.4 22.1 %copy-start.6 = (bf16[256,128]{1,0:T(8,128)(2,1)S(1)}, bf16[256,128]{1,0:T(8,128)(2,1)}, u32[]{:S(2)}) copy-start(bf16[256,128]{1,0:T(8,128)(2,1)} %param.17) | copy-start | bytes 196612
  23.5 32.7 %all-to-all-start = ((bf16[32,2,1024]{2,1,0:T(2,128)(2,1)}), bf16[32,2,1024]{2,1,0:T(2,128)(2,1)S(1)}, u32[]{:S(2)}, u32[]{:S(2)}) async-start(bf16[32,2,1024]{2,1,0:T(2,128)(2,1)} %reshape.656), calls=%async_computation | async-start | bytes 262144 | tf_op jit(solution)/shard_map/all_to_all | solution.py:179
  44.3 1.2 copy-start.3
  44.3 13.7 %copy-start.9 = (f32[2,1]{0,1:T(1,128)}, f32[2,1]{0,1:T(1,128)S(1)}, u32[]{:S(2)}) copy-start(f32[2,1]{0,1:T(1,128)S(1)} %get-tuple-element.178) | copy-start | bytes 28
  58.0 7.5 %copy-start.11 = (f32[1,128]{1,0:T(1,128)S(1)}, f32[1,128]{1,0:T(1,128)}, u32[]{:S(2)}) copy-start(f32[1,128]{1,0:T(1,128)} %pad_bitcast_fusion.1) | copy-start | bytes 1540
  58.0 33.7 %all-to-all-start.1 = ((bf16[16,32,1,2048]{3,1,2,0:T(8,128)(2,1)}), bf16[16,32,1,2048]{3,1,2,0:T(8,128)(2,1)S(1)}, u32[]{:S(2)}, u32[]{:S(2)}) async-start(bf16[16,32,1,2048]{3,1,2,0:T(8,128)(2,1)} %broadcast_in_dim.33), calls=%async_computation.1 | async-start | bytes 4194304 | tf_op jit(solution)/shard_map/all_to_all | solution.py:64
  65.5 67.8 %all-gather.12.cloned.1.call-start = ((), (), s32[]{:S(2)}) async-start(), calls=%async_computation.5 | async-start | bytes 1183744 | tf_op jit(solution)/shard_map/all_gather | solution.py:26
  71.3 133.9 %all-gather.10.cloned.1.call-start = ((), (), s32[]{:S(2)}) async-start(), calls=%async_computation.4 | async-start | bytes 4456448 | tf_op jit(solution)/shard_map/all_gather | solution.py:186
  91.7 1.2 copy-start.12
  94.4 54.2 %copy-start.7 = (bf16[256,128]{1,0:T(8,128)(2,1)S(1)}, bf16[256,128]{1,0:T(8,128)(2,1)}, u32[]{:S(2)}) copy-start(bf16[256,128]{1,0:T(8,128)(2,1)} %param.18) | copy-start | bytes 196612
  94.4 110.8 %copy-start.13 = (bf16[1,4096,128]{2,1,0:T(8,128)(2,1)S(1)}, bf16[1,4096,128]{2,1,0:T(8,128)(2,1)}, u32[]{:S(2)}) copy-start(bf16[1,4096,128]{2,1,0:T(8,128)(2,1)} %param.27) | copy-start | bytes 3145732
  94.4 144.5 %all-gather.8.cloned.1.call-start = ((), (), s32[]{:S(2)}) async-start(), calls=%async_computation.3 | async-start | bytes 1310720 | tf_op jit(solution)/shard_map/all_gather | solution.py:52
  162.1 59.7 %copy-start.8 = (f32[256,2]{0,1:T(2,128)S(1)}, f32[256,2]{0,1:T(2,128)}, u32[]{:S(2)}) copy-start(f32[256,2]{0,1:T(2,128)} %param.24) | copy-start | bytes 6148
  162.2 76.7 %copy-start.2 = (bf16[2048,128]{1,0:T(8,128)(2,1)S(1)}, bf16[2048,128]{1,0:T(8,128)(2,1)}, u32[]{:S(2)}) copy-start(bf16[2048,128]{1,0:T(8,128)(2,1)} %param.20) | copy-start | bytes 1572868
  209.3 31.9 %all-to-all-start.2 = ((bf16[32,16,128]{2,1,0:T(8,128)(2,1)}), bf16[32,16,128]{2,1,0:T(8,128)(2,1)S(1)}, u32[]{:S(2)}, u32[]{:S(2)}) async-start(bf16[32,16,128]{2,1,0:T(8,128)(2,1)} %copy.58), calls=%async_computation.2 | async-start | bytes 262144 | tf_op jit(solution)/shard_map/all_to_all | solution.py:190
Sparse Core Ops, SparseCore 0:
  71.4 61.8 all-gather.11
  136.3 68.8 all-gather.9
  207.3 31.5 all-gather.7
where the time goes:
time: 251 us; the launch traced here: 250 us
  waiting for transfers between devices  128 us (51%)
  starting transfers between devices  35.6 us (14%)
  other arithmetic  24.8 us (10%)
  local copies, waits for them, and re-layouts  18.7 us (7%)
  between operations  18 us (7%)
  blocking collectives  15.3 us (6%)
  matrix products  9.84 us (4%)
    all_gather x1, waiting for transfers between devices, expert_half(): lax.all_gather(hidden, TP, axis=2, tiled=True)  43 us
    all_gather x1, waiting for transfers between devices, collected_together(): both, at, found = (lax.all_gather(jnp.concatenate(lines), axis), 0, {})  36.7 us
    all_to_all x1, waiting for transfers between devices, copy_for_each(): lax.all_to_all(jnp.broadcast_to(array[None], (peers, *array.shape)), axis...  20.4 us
    all_gather x1, waiting for transfers between devices, whole_of(): array = lax.all_gather(array, axis, axis=dim, tiled=True)  16.8 us
    all_to_all x1, starting transfers between devices, expert_half(): lax.all_to_all(own_share, EP, split_axis=0, concat_axis=0, tiled=True)  15.5 us
    all_gather x1, blocking collectives, whole_of(): array = lax.all_gather(array, axis, axis=dim, tiled=True)  13.4 us
    all_to_all x1, starting transfers between devices, expert_half(): lax.all_to_all(expert_out, EP, split_axis=0, concat_axis=0, tiled=True)  12.6 us
    mul x1, other arithmetic, retention_half(): entering = before + jnp.exp(leading)[:, :, None, None] * incoming[1][None]  11.5 us
  transfers between devices with their start and end apart: 6, of which 5 were waited for; matrix products, arithmetic and copies ran while one was open for 13% of the time, Pallas kernels for 0%

commit v1 on v0

--- a/solution.py
+++ b/solution.py
@@ -183,7 +183,7 @@
     hidden = (jax.nn.silu(gate_part) * up_part).astype(jnp.bfloat16)
     expert_out = jnp.einsum(
         "scf,fd->scd",
-        lax.all_gather(hidden, TP, axis=2, tiled=True),
+        jnp.concatenate(lax.all_gather(hidden, TP), axis=2),
         w_down,
         preferred_element_type=jnp.float32,
     ).astype(jnp.bfloat16)

time: 251 us -> 260 us (1.036)
  local copies, waits for them, and re-layouts: 18.7 us -> 33.9 us
  waiting for transfers between devices: 128 us -> 123 us
    all_gather x1, waiting for transfers between devices: 16.8 us -> 1.73 us  [whole_of(): array = lax.all_gather(array, axis, axis=dim, tiled=True)]
    all_to_all x1, waiting for transfers between devices: 0.01 us -> 13 us  [expert_half(): lax.all_to_all(expert_out, EP, split_axis=0, concat_axis=0, tiled=True)]
    all_gather x0 -> x1, local copies, waits for them, and re-layouts: none -> 7.58 us  [expert_half(): lax.all_gather(hidden, TP)]
    reshape x0 -> x1, local copies, waits for them, and re-layouts: none -> 7.5 us  [expert_half(): jnp.concatenate(lax.all_gather(hidden, TP), axis=2)]
    all_gather x1, waiting for transfers between devices: 43 us -> 40.4 us  [expert_half(): lax.all_gather(hidden, TP)]
  transfers between devices with their start and end apart: 6 -> 6, of which waited for: 5 -> 6; matrix products, arithmetic and copies ran while one was open for 13% -> 18% of each run, Pallas kernels for 0% -> 0%
where the time goes in v1:
time: 260 us; the launch traced here: 259 us
  waiting for transfers between devices  123 us (47%)
  starting transfers between devices  35.7 us (14%)
  local copies, waits for them, and re-layouts  33.9 us (13%)
  other arithmetic  24.7 us (10%)
  between operations  18.1 us (7%)
  blocking collectives  14.6 us (6%)
  matrix products  8.96 us (3%)
    all_gather x1, waiting for transfers between devices, expert_half(): lax.all_gather(hidden, TP)  40.4 us
    all_gather x1, waiting for transfers between devices, collected_together(): both, at, found = (lax.all_gather(jnp.concatenate(lines), axis), 0, {})  36.6 us
    all_to_all x1, waiting for transfers between devices, copy_for_each(): lax.all_to_all(jnp.broadcast_to(array[None], (peers, *array.shape)), axis...  20.4 us
    all_to_all x1, starting transfers between devices, expert_half(): lax.all_to_all(own_share, EP, split_axis=0, concat_axis=0, tiled=True)  15.5 us
    all_to_all x1, waiting for transfers between devices, expert_half(): lax.all_to_all(expert_out, EP, split_axis=0, concat_axis=0, tiled=True)  13 us
    all_gather x1, blocking collectives, whole_of(): array = lax.all_gather(array, axis, axis=dim, tiled=True)  12.7 us
    all_to_all x1, starting transfers between devices, expert_half(): lax.all_to_all(expert_out, EP, split_axis=0, concat_axis=0, tiled=True)  12.6 us
    mul x1, other arithmetic, retention_half(): entering = before + jnp.exp(leading)[:, :, None, None] * incoming[1][None]  11.5 us
  transfers between devices with their start and end apart: 6, of which 6 were waited for; matrix products, arithmetic and copies ran while one was open for 18% of the time, Pallas kernels for 0%

profile of v1, /device:TPU:2, one launch (start us, length us, event | category | flops | bytes accessed | tf_op | source)
XLA Modules:
  0.0 258.8 jit_solution(13104135569204509674)
XLA Ops:
  7.2 1.0 copy.47
  8.2 0.1 eq.29
  8.3 0.1 eq.25
  8.4 0.7 broadcast_multiply_fusion
  9.1 1.2 reduce-window.18
  10.3 0.2 slice_reduce_fusion
  10.6 0.1 copy.46
  10.7 0.1 mul.536
  11.0 2.4 scatter_custom_fusion
  13.5 0.7 convert_element_type.89
  14.2 1.5 fusion
  15.7 0.3 fusion.2
  16.0 3.3 %gather_fusion = bf16[512,2048]{1,0:T(8,128)(2,1)} fusion(bf16[256,2048]{1,0:T(8,128)(2,1)S(1)} %fusion.2, s32[1024]{0:T(1024)S(1)} %pad_clamp_fusion.1), kind=kCustom, calls=%fused_computation | custom fusion | bytes 4196352 | tf_op jit(solution)/shard_map/gather | solution.py:173
  19.4 1.5 constant_dynamic-slice_fusion.1
  20.9 0.5 broadcast.370
  21.4 1.4 reduce.10
  22.8 0.7 reshape.665
  23.5 15.5 %all-to-all-start = ((bf16[32,2,1024]{2,1,0:T(2,128)(2,1)}), bf16[32,2,1024]{2,1,0:T(2,128)(2,1)S(1)}, u32[]{:S(2)}, u32[]{:S(2)}) async-start(bf16[32,2,1024]{2,1,0:T(2,128)(2,1)} %reshape.665), calls=%async_computation | async-start | bytes 262144 | tf_op jit(solution)/shard_map/all_to_all | solution.py:179
  39.1 0.1 copy.43
  39.2 0.2 reduce_window_sum.33
  39.4 0.6 slice_reduce_fusion.1
  40.2 0.6 fusion.33
  40.8 0.1 fusion.38
  40.9 0.6 fusion.79
  41.5 0.4 convolution_bitcast_fusion.1
  41.9 2.4 while.13
  41.9 0.6 fusion.87
  42.5 0.6 bitcast_add_fusion.2
  43.1 0.6 fusion.87
  43.7 0.6 bitcast_add_fusion.2
  44.9 0.5 pad_bitcast_fusion.1
  45.5 10.7 %all-to-all-done = bf16[32,2,1024]{2,1,0:T(2,128)(2,1)S(1)} async-done(((bf16[32,2,1024]{2,1,0:T(2,128)(2,1)}), bf16[32,2,1024]{2,1,0:T(2,128)(2,1)S(1)}, u32[]{:S(2)}, u32[]{:S(2)}) %all-to-all-start) | async-done | bytes 131104 | tf_op jit(solution)/shard_map/all_to_all | solution.py:179
  56.4 1.6 broadcast_in_dim.33
  58.0 7.5 %all-to-all-start.1 = ((bf16[16,32,1,2048]{3,1,2,0:T(8,128)(2,1)}), bf16[16,32,1,2048]{3,1,2,0:T(8,128)(2,1)S(1)}, u32[]{:S(2)}, u32[]{:S(2)}) async-start(bf16[16,32,1,2048]{3,1,2,0:T(8,128)(2,1)} %broadcast_in_dim.33), calls=%async_computation.1 | async-start | bytes 4194304 | tf_op jit(solution)/shard_map/all_to_all | solution.py:64
  65.6 1.9 all-gather.3
  67.5 0.6 fusion.78
  70.0 0.7 fusion.65
  70.6 0.6 maximum_bitcast_fusion.1
  71.3 20.4 %all-to-all-done.1 = bf16[16,32,1,2048]{3,1,2,0:T(8,128)(2,1)S(1)} async-done(((bf16[16,32,1,2048]{3,1,2,0:T(8,128)(2,1)}), bf16[16,32,1,2048]{3,1,2,0:T(8,128)(2,1)S(1)}, u32[]{:S(2)}, u32[]{:S(2)}) %all-to-all-start.1) | async-done | bytes 2097184 | tf_op jit(solution)/shard_map/all_to_all | solution.py:64
  91.7 0.7 fusion.5
  92.5 0.5 copy-done.14
  92.9 0.7 fusion.10
  93.7 0.8 copy.51
  94.6 0.8 reduce-window.14
  96.1 0.6 fusion.71
  96.7 36.6 %all-gather.13.cloned.1.call-done = f32[16,129,128]{2,1,0:T(8,128)} async-done(((f32[1,129,128]{2,1,0:T(8,128)}), f32[16,129,128]{2,1,0:T(8,128)}) %all-gather.13.cloned.1.call-update) | async-done | bytes 1056784 | tf_op jit(solution)/shard_map/all_gather | solution.py:26
  133.3 0.8 slice.250
  134.1 0.6 fusion.77
  135.4 11.5 %fusion.56 = f32[128,128]{1,0:T(8,128)S(1)} fusion(f32[16,129,128]{2,1,0:T(8,128)} %all-gather.13.cloned.1.call-done, f32[2,129,128]{2,1,0:T(8,128)S(1)} %all-gather.3, f32[]{:T(128)} %bitcast.46, f32[]{:T(128)} %bitcast.45, f32[]{:T(128)} %bitcast.44, f32[]{:T(128)} %bitcast.43, f32[]{:T(128)} %bitcast.42, f32[]{:T(128)} %bitcast.41, f32[]{:T(128)} %bitcast.40, ...), kind=kLoop, calls=%fused_computation.81 | loop fusion | flops 884736 | bytes 1245278 | tf_op jit(solution)/shard_map/mul | solution.py:136
  146.9 0.3 fusion.14
  147.2 0.4 fusion.39
  147.7 0.1 fusion.49
  147.8 12.7 %all_gather.28 = bf16[256,512]{1,0:T(8,128)(2,1)} all-gather(bf16[256,128]{1,0:T(8,128)(2,1)S(1)} %fusion.49), channel_id=1, replica_groups=mesh['ep_0'=16,'ep_1'=2,'tp_0'=4,'tp_1'=4] {'tp_1'}, dimensions={1}, use_global_device_ids=true | all-gather | bytes 327680 | tf_op jit(solution)/shard_map/all_gather | solution.py:52
  160.5 40.4 %all-gather.11.cloned.1.call-done = bf16[512,16,256]{2,1,0:T(8,128)(2,1)} async-done(((bf16[32,16,256]{2,1,0:T(8,128)(2,1)}), bf16[512,16,256]{2,1,0:T(8,128)(2,1)}) %all-gather.11.cloned.1.call-update) | async-done | bytes 4194320 | tf_op jit(solution)/shard_map/all_gather | solution.py:186
  200.9 7.6 %copy.60 = bf16[16,32,16,256]{3,0,2,1:T(8,128)(2,1)} copy(bf16[16,32,16,256]{3,2,1,0:T(8,128)(2,1)} %bitcast.165) | data formatting | bytes 8388608 | tf_op jit(solution)/shard_map/all_gather | solution.py:186
  208.4 7.5 %reshape.615 = bf16[32,16,4096]{2,1,0:T(8,128)(2,1)} reshape(bf16[32,16,16,256]{3,2,1,0:T(8,128)(2,1)} %bitcast.162) | data formatting | bytes 8388608 | tf_op jit(solution)/shard_map/reshape | solution.py:186
  215.9 4.1 %convolution_convert_fusion = bf16[32,16,128]{2,1,0:T(8,128)(2,1)} fusion(bf16[32,16,4096]{2,1,0:T(8,128)(2,1)} %reshape.615, bf16[1,4096,128]{2,1,0:T(8,128)(2,1)S(1)} %copy-done.15), kind=kOutput, calls=%fused_computation.18 | convolution fusion | flops 536936448 | bytes 5373952 | tf_op jit(solution)/shard_map/scf,fd->scd/dot_general | solution.py:184
  220.1 12.6 %all-to-all-start.2 = ((bf16[32,16,128]{2,1,0:T(8,128)(2,1)}), bf16[32,16,128]{2,1,0:T(8,128)(2,1)S(1)}, u32[]{:S(2)}, u32[]{:S(2)}) async-start(bf16[32,16,128]{2,1,0:T(8,128)(2,1)} %convolution_convert_fusion), calls=%async_computation.2 | async-start | bytes 262144 | tf_op jit(solution)/shard_map/all_to_all | solution.py:190
  232.7 0.1 copy.53
  232.8 1.7 all-gather.9.cloned.1.call-done
  234.6 2.3 convolution_convert_fusion.1
  236.9 13.0 %all-to-all-done.2 = bf16[32,16,128]{2,1,0:T(8,128)(2,1)S(1)} async-done(((bf16[32,16,128]{2,1,0:T(8,128)(2,1)}), bf16[32,16,128]{2,1,0:T(8,128)(2,1)S(1)}, u32[]{:S(2)}, u32[]{:S(2)}) %all-to-all-start.2) | async-done | bytes 131104 | tf_op jit(solution)/shard_map/all_to_all | solution.py:190
  249.9 1.3 gather_fusion.1
  251.2 1.1 fusion.19
  (62 shorter events, 0.8 us)
Async XLA Ops:
  7.2 84.6 %copy-start = (bf16[1,2048,256]{2,1,0:T(8,128)(2,1)S(1)}, bf16[1,2048,256]{2,1,0:T(8,128)(2,1)}, u32[]{:S(2)}) copy-start(bf16[1,2048,256]{2,1,0:T(8,128)(2,1)} %param.25) | copy-start | bytes 3145732
  7.2 8.5 %copy-start.1 = (bf16[256,2048]{1,0:T(8,128)(2,1)S(1)}, bf16[256,2048]{1,0:T(8,128)(2,1)}, u32[]{:S(2)}) copy-start(bf16[256,2048]{1,0:T(8,128)(2,1)} %param.21) | copy-start | bytes 3145732
  16.0 23.1 %copy-start.12 = (f32[256,1]{0,1:T(1,128)S(1)}, f32[256,1]{0,1:T(1,128)}, u32[]{:S(2)}) copy-start(f32[256,1]{0,1:T(1,128)} %param.19) | copy-start | bytes 3076
  16.0 24.1 %copy-start.5 = (bf16[256,128]{1,0:T(8,128)(2,1)S(1)}, bf16[256,128]{1,0:T(8,128)(2,1)}, u32[]{:S(2)}) copy-start(bf16[256,128]{1,0:T(8,128)(2,1)} %param.16) | copy-start | bytes 196612
  16.0 24.1 %copy-start.6 = (bf16[256,128]{1,0:T(8,128)(2,1)S(1)}, bf16[256,128]{1,0:T(8,128)(2,1)}, u32[]{:S(2)}) copy-start(bf16[256,128]{1,0:T(8,128)(2,1)} %param.15) | copy-start | bytes 196612
  19.4 22.1 %copy-start.7 = (bf16[256,128]{1,0:T(8,128)(2,1)S(1)}, bf16[256,128]{1,0:T(8,128)(2,1)}, u32[]{:S(2)}) copy-start(bf16[256,128]{1,0:T(8,128)(2,1)} %param.17) | copy-start | bytes 196612
  23.5 32.7 %all-to-all-start = ((bf16[32,2,1024]{2,1,0:T(2,128)(2,1)}), bf16[32,2,1024]{2,1,0:T(2,128)(2,1)S(1)}, u32[]{:S(2)}, u32[]{:S(2)}) async-start(bf16[32,2,1024]{2,1,0:T(2,128)(2,1)} %reshape.665), calls=%async_computation | async-start | bytes 262144 | tf_op jit(solution)/shard_map/all_to_all | solution.py:179
  44.3 13.8 %copy-start.3 = (f32[2,1,128,128]{3,2,1,0:T(8,128)}, f32[2,1,128,128]{3,2,1,0:T(8,128)S(1)}, u32[]{:S(2)}) copy-start(f32[2,1,128,128]{3,2,1,0:T(8,128)S(1)} %get-tuple-element.30) | copy-start | bytes 393220
  44.3 13.7 %copy-start.11 = (f32[2,1]{0,1:T(1,128)}, f32[2,1]{0,1:T(1,128)S(1)}, u32[]{:S(2)}) copy-start(f32[2,1]{0,1:T(1,128)S(1)} %get-tuple-element.179) | copy-start | bytes 28
  58.0 7.5 %copy-start.13 = (f32[1,128]{1,0:T(1,128)S(1)}, f32[1,128]{1,0:T(1,128)}, u32[]{:S(2)}) copy-start(f32[1,128]{1,0:T(1,128)} %pad_bitcast_fusion.1) | copy-start | bytes 1540
  58.0 33.7 %all-to-all-start.1 = ((bf16[16,32,1,2048]{3,1,2,0:T(8,128)(2,1)}), bf16[16,32,1,2048]{3,1,2,0:T(8,128)(2,1)S(1)}, u32[]{:S(2)}, u32[]{:S(2)}) async-start(bf16[16,32,1,2048]{3,1,2,0:T(8,128)(2,1)} %broadcast_in_dim.33), calls=%async_computation.1 | async-start | bytes 4194304 | tf_op jit(solution)/shard_map/all_to_all | solution.py:64
  65.5 67.8 %all-gather.13.cloned.1.call-start = ((), (), s32[]{:S(2)}) async-start(), calls=%async_computation.5 | async-start | bytes 1183744 | tf_op jit(solution)/shard_map/all_gather | solution.py:26
  71.3 129.6 %all-gather.11.cloned.1.call-start = ((), (), s32[]{:S(2)}) async-start(), calls=%async_computation.4 | async-start | bytes 4456448 | tf_op jit(solution)/shard_map/all_gather | solution.py:186
  91.7 1.2 copy-start.14
  93.7 53.2 %copy-start.4 = (f32[2,1,128,128]{3,2,1,0:T(8,128)S(1)}, f32[2,1,128,128]{3,2,1,0:T(8,128)}, u32[]{:S(2)}) copy-start(f32[2,1,128,128]{3,2,1,0:T(8,128)} %copy-done.3) | copy-start | bytes 393220
  93.7 53.2 %copy-start.9 = (f32[2,128]{1,0:T(2,128)S(1)}, f32[2,128]{1,0:T(2,128)}, u32[]{:S(2)}) copy-start(f32[2,128]{1,0:T(2,128)} %get-tuple-element.106) | copy-start | bytes 3076
  93.7 54.0 %copy-start.8 = (bf16[256,128]{1,0:T(8,128)(2,1)S(1)}, bf16[256,128]{1,0:T(8,128)(2,1)}, u32[]{:S(2)}) copy-start(bf16[256,128]{1,0:T(8,128)(2,1)} %param.18) | copy-start | bytes 196612
  94.6 140.0 %all-gather.9.cloned.1.call-start = ((), (), s32[]{:S(2)}) async-start(), calls=%async_computation.3 | async-start | bytes 1310720 | tf_op jit(solution)/shard_map/all_gather | solution.py:52
  208.4 7.5 %copy-start.15 = (bf16[1,4096,128]{2,1,0:T(8,128)(2,1)S(1)}, bf16[1,4096,128]{2,1,0:T(8,128)(2,1)}, u32[]{:S(2)}) copy-start(bf16[1,4096,128]{2,1,0:T(8,128)(2,1)} %param.27) | copy-start | bytes 3145732
  215.9 16.7 %copy-start.10 = (f32[256,2]{0,1:T(2,128)S(1)}, f32[256,2]{0,1:T(2,128)}, u32[]{:S(2)}) copy-start(f32[256,2]{0,1:T(2,128)} %param.24) | copy-start | bytes 6148
  215.9 18.6 %copy-start.2 = (bf16[2048,128]{1,0:T(8,128)(2,1)S(1)}, bf16[2048,128]{1,0:T(8,128)(2,1)}, u32[]{:S(2)}) copy-start(bf16[2048,128]{1,0:T(8,128)(2,1)} %param.20) | copy-start | bytes 1572868
  220.1 29.8 %all-to-all-start.2 = ((bf16[32,16,128]{2,1,0:T(8,128)(2,1)}), bf16[32,16,128]{2,1,0:T(8,128)(2,1)S(1)}, u32[]{:S(2)}, u32[]{:S(2)}) async-start(bf16[32,16,128]{2,1,0:T(8,128)(2,1)} %convolution_convert_fusion), calls=%async_computation.2 | async-start | bytes 262144 | tf_op jit(solution)/shard_map/all_to_all | solution.py:190
Sparse Core Ops, SparseCore 0:
  71.4 61.8 all-gather.12
  136.3 64.5 all-gather.10
  203.0 31.5 all-gather.8
